TPU v7x, 256 devices: a whole 4x4x8 slice. The times are simulated.
256 devices in a mesh: ep: 16 (over y, x), tp: 16 (over z, core).
Axes of the slice: x: 4, y: 4, z: 8, core: 2. Of those that a mesh axis runs over, the one named last changes fastest.
Arguments:
- tokens: bfloat16 [65536, 2048], P(('ep', 'tp')), may hold values from -6 to 6
- norm_gain: float32 [2048], replicated, may hold values from 0.1 to 1.9
- expert_ids: int32 [65536, 2], P(('ep', 'tp')), may hold values from 0 to 15, all different within a row; in each aligned block of 256 rows (0 to 255, 256 to 511, ...) at most 64 rows name the same one
- gate_weights: float32 [65536, 2], P(('ep', 'tp')), may hold values from 0.2 to 1
- w_gate: bfloat16 [16, 2048, 1024], P('ep', None, 'tp'), may hold values from -0.125 to 0.125
- w_up: bfloat16 [16, 2048, 1024], P('ep', None, 'tp'), may hold values from -0.125 to 0.125
- w_down: bfloat16 [16, 2048, 1024], P('ep', None, 'tp'), may hold values from -0.1875 to 0.1875
- dense_gate: bfloat16 [2048, 256], P('ep'), may hold values from -0.125 to 0.125
- dense_up: bfloat16 [2048, 256], P('ep'), may hold values from -0.125 to 0.125
- dense_down: bfloat16 [256, 2048], P(None, 'ep'), may hold values from -0.375 to 0.375
- mix_vector: float32 [2048], replicated, may hold values from -0.125 to 0.125
Outputs:
- mixed: bfloat16 [65536, 2048], P(('ep', 'tp'))
Inputs may be any that keep to these rules, and one draw needn't show every extreme that they name: `expert_ids`: A row names 2 different experts. In the rows of one device (aligned blocks of 256 rows) each expert is named by at most 64 rows, a bound that some block reaches.
All inputs are finite; a program needn't handle non-finite values.
Results may differ from a plain program's by a relative error of at most 0.0075.
Values may be sent and summed in bfloat16 or wider, within the bound.
No kernel may reach another device: no remote copies, remote signals or barrier semaphores. Data moves between devices by JAX's collectives and lax.ppermute only.
A program may use at most 320 MiB of HBM per device.

v0:
```python
import jax
import jax.numpy as jnp
from jax import lax
from jax.sharding import Mesh
from jax.sharding import PartitionSpec as P

EP = ("ep_0", "ep_1")
EP_TP = ("ep_0", "ep_1", "tp")


eps = 1e-06


def in_one_piece(arrays, axis, dim, along):
    widths = [a.shape[along] for a in arrays]
    both = jnp.concatenate(arrays, axis=along)
    out = lax.all_gather(both, axis, axis=dim, tiled=True)
    return tuple(jnp.split(out, [sum(widths[:k]) for k in range(1, len(widths))], axis=along))


def whole_of(x, axes, dim):
    if not axes:
        return x
    nearer = lax.all_gather(x, axes[-1], axis=dim, tiled=True)
    return whole_of(nearer, axes[:-1], dim)


def gather_turned(arrays, axis, dims):
    turned = [jnp.moveaxis(a, dim, 0) for a, dim in zip(arrays, dims)]
    both = jnp.concatenate([t.reshape(len(t), -1) for t in turned], axis=1)
    out, at, gathered = (lax.all_gather(both, axis, axis=0, tiled=True), 0, [])
    for t, dim in zip(turned, dims):
        piece = out[:, at : at + t[0].size].reshape(-1, *t.shape[1:])
        gathered.append(jnp.moveaxis(piece, 0, dim))
        at += t[0].size
    return tuple(gathered)


def dense_branch(normed, dense_gate, dense_up, dense_down, mix_vector):
    pieces = in_one_piece((dense_gate, dense_up), EP, 0, 1)
    dense_g = jnp.dot(normed, pieces[0], preferred_element_type=jnp.float32)
    dense_u = jnp.dot(normed, pieces[1], preferred_element_type=jnp.float32)
    dense_hidden = (jax.nn.silu(dense_g) * dense_u).astype(jnp.bfloat16)
    dense_out = jnp.dot(
        dense_hidden, whole_of(dense_down, EP, 1), preferred_element_type=jnp.float32
    )
    mix = jax.nn.sigmoid(jnp.sum(normed.astype(jnp.float32) * mix_vector, axis=1))
    return mix[:, None] * dense_out


def on_device(
    tokens,
    norm_gain,
    expert_ids,
    gate_weights,
    w_gate,
    w_up,
    w_down,
    dense_gate,
    dense_up,
    dense_down,
    mix_vector,
):
    values = tokens.astype(jnp.float32)
    scale = lax.rsqrt(jnp.mean(values * values, axis=1, keepdims=True) + eps)
    normed = (values * scale * norm_gain).astype(jnp.bfloat16)
    count_tok, topk = expert_ids.shape
    width = tokens.shape[1]
    groups = lax.axis_size(EP)
    capacity = 2 * count_tok * topk // groups
    flat_ids = expert_ids.reshape(-1)
    onehot = (flat_ids[:, None] == jnp.arange(groups, dtype=jnp.int32)[None, :]).astype(jnp.int32)
    before = jnp.cumsum(onehot, axis=0) - onehot
    slot = jnp.sum(before * onehot, axis=1)
    dest = flat_ids * capacity + slot
    owner = jnp.arange(count_tok * topk, dtype=jnp.int32) // topk
    buffer = jnp.zeros((groups * capacity, width), jnp.bfloat16).at[dest].set(normed[owner])
    arrived = lax.all_to_all(
        buffer.reshape(groups, capacity, width), EP, split_axis=0, concat_axis=0, tiled=True
    )
    rows = arrived.reshape(groups * capacity, width)
    pieces = gather_turned((w_gate, w_up, w_down), "tp", (2, 2, 2))
    gate = jnp.dot(rows, pieces[0][0], preferred_element_type=jnp.float32)
    upper = jnp.dot(rows, pieces[1][0], preferred_element_type=jnp.float32)
    hidden = (jax.nn.silu(gate) * upper).astype(jnp.bfloat16)
    expert_out = lax.dot_general(
        hidden, pieces[2][0], (((1,), (1,)), ((), ())), preferred_element_type=jnp.float32
    )
    results = expert_out.astype(jnp.bfloat16).reshape(groups, capacity, width)
    returned = lax.all_to_all(results, EP, split_axis=0, concat_axis=0, tiled=True)
    picked = returned.reshape(groups * capacity, width)[dest].reshape(count_tok, topk, width)
    routed = jnp.einsum("tk,tkd->td", gate_weights, picked.astype(jnp.float32))
    side = dense_branch(normed, dense_gate, dense_up, dense_down, mix_vector)
    return (routed + side).astype(jnp.bfloat16)


def solution(mesh):
    torus = Mesh(mesh.devices.reshape(4, 4, mesh.shape["tp"]), ("ep_0", "ep_1", "tp"))
    return jax.shard_map(
        on_device,
        mesh=torus,
        in_specs=(
            P(EP_TP, None),
            P(),
            P(EP_TP, None),
            P(EP_TP, None),
            P(EP, None, "tp"),
            P(EP, None, "tp"),
            P(EP, None, "tp"),
            P(EP, None),
            P(EP, None),
            P(None, EP),
            P(),
        ),
        out_specs=P(EP_TP, None),
        check_vma=False,
    )
```

profile of v0, /device:TPU:2, one launch (start us, length us, event | category | flops | bytes accessed | tf_op | source)
XLA Modules:
  0.0 238.7 jit_solution(1675348689646870334)
XLA Ops:
  6.5 2.1 pad_maximum_fusion
  8.9 0.1 eq.29
  9.0 0.1 eq.25
  9.2 1.2 reduce-window.6
  10.3 0.2 slice_reduce_fusion
  10.6 0.1 copy.12
  10.7 0.1 mul.70
  11.0 0.3 fusion.6
  11.3 0.5 multiply_reduce_fusion
  11.9 12.8 %scatter_custom_fusion = bf16[1024,2048]{1,0:T(8,128)(2,1)} fusion(s32[512]{0:T(512)S(1)} %bitcast.77, bf16[256,2048]{1,0:T(8,128)(2,1)S(1)} %get-tuple-element.6, s32[1024]{0:T(1024)S(1)} %pad_clamp_fusion.1, bf16[]{:T(256)} %constant.32.clone.1), kind=kCustom, calls=%fused_computation.19 | custom fusion | bytes 4194306 | tf_op jit(solution)/shard_map/scatter | solution.py:77
  24.7 7.6 %all-to-all-start = ((bf16[16,64,2048]{2,1,0:T(8,128)(2,1)}), bf16[16,64,2048]{2,1,0:T(8,128)(2,1)}, u32[]{:S(2)}, u32[]{:S(2)}) async-start(bf16[16,64,2048]{2,1,0:T(8,128)(2,1)} %bitcast.72), calls=%async_computation | async-start | bytes 8388608 | tf_op jit(solution)/shard_map/all_to_all | solution.py:78
  32.4 0.7 pad_maximum_fusion.1
  33.0 58.4 %all-to-all-done = bf16[16,64,2048]{2,1,0:T(8,128)(2,1)} async-done(((bf16[16,64,2048]{2,1,0:T(8,128)(2,1)}), bf16[16,64,2048]{2,1,0:T(8,128)(2,1)}, u32[]{:S(2)}, u32[]{:S(2)}) %all-to-all-start) | async-done | bytes 4194336 | tf_op jit(solution)/shard_map/all_to_all | solution.py:78
  91.5 10.0 %fusion.1 = f32[1024,1024]{1,0:T(8,128)} fusion(bf16[1024,2048]{1,0:T(8,128)(2,1)} %bitcast.5, bf16[1024,6144]{1,0:T(8,128)(2,1)} %all-gather.4.cloned.1.call-done), kind=kOutput, calls=%fused_computation.6 | convolution fusion | flops 4294967296 | bytes 12582912 | tf_op jit(solution)/shard_map/dot_general | solution.py:84
  101.4 15.5 %fusion.3 = bf16[1024,2048]{1,0:T(8,128)(2,1)} fusion(bf16[1024,6144]{1,0:T(8,128)(2,1)} %all-gather.4.cloned.1.call-done, f32[1024,1024]{1,0:T(8,128)} %fusion.1, bf16[1024,2048]{1,0:T(8,128)(2,1)} %bitcast.5), kind=kOutput, calls=%fused_computation.10 | convolution fusion | flops 8598323200 | bytes 20971520 | tf_op jit(solution)/shard_map/dot_general | solution.py:86
  117.0 9.0 %all-to-all-start.1 = ((bf16[16,64,2048]{2,1,0:T(8,128)(2,1)}), bf16[16,64,2048]{2,1,0:T(8,128)(2,1)}, u32[]{:S(2)}, u32[]{:S(2)}) async-start(bf16[16,64,2048]{2,1,0:T(8,128)(2,1)} %bitcast.73), calls=%async_computation.1 | async-start | bytes 8388608 | tf_op jit(solution)/shard_map/all_to_all | solution.py:90
  126.0 75.2 %all_gather.14 = bf16[256,512]{1,0:T(8,128)(2,1)} all-gather(bf16[256,128]{1,0:T(8,128)(2,1)S(1)} %copy-done.1), channel_id=1, replica_groups=mesh['ep_0'=4,'ep_1'=4,'tp'=16] {'ep_1'}, dimensions={1}, use_global_device_ids=true | all-gather | bytes 327680 | tf_op jit(solution)/shard_map/all_gather | solution.py:24
  201.3 0.2 copy.16
  201.5 1.7 fusion.15
  203.2 7.1 %gather_fusion = bf16[512,2048]{1,0:T(8,128)(2,1)S(1)} fusion(bf16[1024,2048]{1,0:T(8,128)(2,1)} %bitcast.22, s32[1024]{0:T(1024)S(1)} %pad_clamp_fusion), kind=kCustom, calls=%fused_computation.1 | custom fusion | bytes 4196352 | tf_op jit(solution)/shard_map/gather | solution.py:91
  210.3 2.6 %reshape.149 = bf16[256,2,2048]{2,1,0:T(2,128)(2,1)} reshape(bf16[512,2048]{1,0:T(8,128)(2,1)S(1)} %gather_fusion) | data formatting | bytes 4194304 | tf_op jit(solution)/shard_map/reshape | solution.py:91
  213.0 5.5 %fusion.30 = f32[256,1,2048]{2,1,0:T(1,128)} fusion(bf16[256,2,2048]{2,1,0:T(2,128)(2,1)} %reshape.149, bf16[256,2,1]{1,2,0:T(2,128)(2,1)S(1)} %copy.16), kind=kOutput, calls=%fused_computation.58 | convolution fusion | flops 2097152 | bytes 4195328 | tf_op jit(solution)/shard_map/tk,tkd->td/dot_general | solution.py:92
  218.4 9.3 %all-gather.8.cloned.1.call-done = bf16[256,2048]{1,0:T(8,128)(2,1)} async-done(((bf16[256,512]{1,0:T(8,128)(2,1)}), bf16[256,2048]{1,0:T(8,128)(2,1)}) %all-gather.8.cloned.1.call-update) | async-done | bytes 1048592 | tf_op jit(solution)/shard_map/all_gather | solution.py:24
  227.8 4.4 %fusion.5 = bf16[256,2048]{1,0:T(8,128)(2,1)} fusion(bf16[256,2048]{1,0:T(8,128)(2,1)} %all-gather.8.cloned.1.call-done, f32[256,1,2048]{2,1,0:T(1,128)} %fusion.30, bf16[256,2048]{1,0:T(8,128)(2,1)S(1)} %get-tuple-element.6, bf16[2048,512]{1,0:T(8,128)(2,1)S(1)} %copy-done.8, f32[256]{0:T(256)S(1)} %add_divide_fusion, f32[256,256]{1,0:T(8,128)S(1)} %fusion.15), kind=kOutput, calls=%fused_computation.15 | convolution fusion | flops 538836992 | bytes 6554624 | tf_op jit(solution)/shard_map/dot_general | solution.py:44
  (39 shorter events, 0.5 us)
Async XLA Ops:
  6.5 2.2 copy-start.6
  6.5 4.5 %copy-start = (bf16[256,2048]{1,0:T(8,128)(2,1)S(1)}, bf16[256,2048]{1,0:T(8,128)(2,1)}, u32[]{:S(2)}) copy-start(bf16[256,2048]{1,0:T(8,128)(2,1)} %param.11) | copy-start | bytes 3145732
  6.5 84.9 %all-gather.4.cloned.1.call-start = ((), (), s32[]{:S(2)}) async-start(), calls=%async_computation.2 | async-start | bytes 13369344 | tf_op jit(solution)/shard_map/all_gather | solution.py:31
  6.5 4.8 %copy-start.4 = (f32[2048]{0:T(1024)S(1)}, f32[2048]{0:T(1024)}, u32[]{:S(2)}) copy-start(f32[2048]{0:T(1024)} %param.21) | copy-start | bytes 24580
  6.5 4.8 %copy-start.5 = (f32[2048]{0:T(1024)S(1)}, f32[2048]{0:T(1024)}, u32[]{:S(2)}) copy-start(f32[2048]{0:T(1024)} %param.12) | copy-start | bytes 24580
  24.7 7.7 %copy-start.2 = (bf16[128,256]{1,0:T(8,128)(2,1)S(1)}, bf16[128,256]{1,0:T(8,128)(2,1)}, u32[]{:S(2)}) copy-start(bf16[128,256]{1,0:T(8,128)(2,1)} %param.19) | copy-start | bytes 196612
  24.7 7.7 %copy-start.3 = (bf16[128,256]{1,0:T(8,128)(2,1)S(1)}, bf16[128,256]{1,0:T(8,128)(2,1)}, u32[]{:S(2)}) copy-start(bf16[128,256]{1,0:T(8,128)(2,1)} %param.18) | copy-start | bytes 196612
  24.7 66.8 %all-to-all-start = ((bf16[16,64,2048]{2,1,0:T(8,128)(2,1)}), bf16[16,64,2048]{2,1,0:T(8,128)(2,1)}, u32[]{:S(2)}, u32[]{:S(2)}) async-start(bf16[16,64,2048]{2,1,0:T(8,128)(2,1)} %bitcast.72), calls=%async_computation | async-start | bytes 8388608 | tf_op jit(solution)/shard_map/all_to_all | solution.py:78
  32.3 169.2 %all-gather.6.cloned.1.call-start = ((), (), s32[]{:S(2)}) async-start(), calls=%async_computation.3 | async-start | bytes 2228224 | tf_op jit(solution)/shard_map/all_gather | solution.py:17
  117.0 9.0 %copy-start.1 = (bf16[256,128]{1,0:T(8,128)(2,1)S(1)}, bf16[256,128]{1,0:T(8,128)(2,1)}, u32[]{:S(2)}) copy-start(bf16[256,128]{1,0:T(8,128)(2,1)} %param.20) | copy-start | bytes 196612
  117.0 84.3 %copy-start.7 = (f32[256,2]{0,1:T(2,128)S(1)}, f32[256,2]{0,1:T(2,128)}, u32[]{:S(2)}) copy-start(f32[256,2]{0,1:T(2,128)} %param.14) | copy-start | bytes 6148
  117.0 86.2 %all-to-all-start.1 = ((bf16[16,64,2048]{2,1,0:T(8,128)(2,1)}), bf16[16,64,2048]{2,1,0:T(8,128)(2,1)}, u32[]{:S(2)}, u32[]{:S(2)}) async-start(bf16[16,64,2048]{2,1,0:T(8,128)(2,1)} %bitcast.73), calls=%async_computation.1 | async-start | bytes 8388608 | tf_op jit(solution)/shard_map/all_to_all | solution.py:90
  125.9 101.8 %all-gather.8.cloned.1.call-start = ((), (), s32[]{:S(2)}) async-start(), calls=%async_computation.4 | async-start | bytes 1310720 | tf_op jit(solution)/shard_map/all_gather | solution.py:24
  213.0 14.8 %copy-start.8 = (bf16[2048,512]{1,0:T(8,128)(2,1)S(1)}, bf16[2048,512]{1,0:T(8,128)(2,1)}, u32[]{:S(2)}) copy-start(bf16[2048,512]{1,0:T(8,128)(2,1)} %all-gather.6.cloned.1.call-done) | copy-start | bytes 6291460
Sparse Core Ops, SparseCore 0:
  9.2 78.5 all-gather.3
  90.2 85.9 all-gather.5
  201.4 26.3 all-gather.7
where the time goes:
time: 239 us
  blocking collectives  75.2 us (31%)
  waiting for transfers between devices  67.9 us (28%)
  matrix products  37 us (15%)
  local copies, waits for them, and re-layouts  23.7 us (10%)
  starting transfers between devices  16.6 us (7%)
  between operations  13.3 us (6%)
  other arithmetic  4.93 us (2%)
    all_gather x1, blocking collectives, whole_of(): nearer = lax.all_gather(x, axes[-1], axis=dim, tiled=True)  75.2 us
    all_to_all x1, waiting for transfers between devices, on_device(): lax.all_to_all(buffer.reshape(groups, capacity, width), EP, split_axis=0,...  58.4 us
    dot_general x1, matrix products, on_device(): lax.dot_general(hidden, pieces[2][0], (((1,), (1,)), ((), ())), preferred...  15.5 us
    scatter x1, local copies, waits for them, and re-layouts, on_device(): jnp.zeros((groups * capacity, width), jnp.bfloat16).at[dest]  12.8 us
    dot_general x1, matrix products, on_device(): upper = jnp.dot(rows, pieces[1][0], preferred_element_type=jnp.float32)  9.96 us
    all_gather x1, waiting for transfers between devices, whole_of(): nearer = lax.all_gather(x, axes[-1], axis=dim, tiled=True)  9.34 us
    all_to_all x1, starting transfers between devices, on_device(): lax.all_to_all(results, EP, split_axis=0, concat_axis=0, tiled=True)  8.96 us
    all_to_all x1, starting transfers between devices, on_device(): lax.all_to_all(buffer.reshape(groups, capacity, width), EP, split_axis=0,...  7.61 us
  transfers between devices with their start and end apart: 5, of which 2 were waited for; matrix products, arithmetic and copies ran while one was open for 25% of the time, Pallas kernels for 0%

commit v1 on v0

v1 whole, which is shorter than its diff:
```python
import functools

import jax
import jax.numpy as jnp
from jax import lax
from jax.experimental import pallas as pl
from jax.experimental.pallas import tpu as pltpu
from jax.sharding import Mesh
from jax.sharding import PartitionSpec as P

EP = ("ep_0", "ep_1")
EP_TP = ("ep_0", "ep_1", "tp")
EPS = 1e-06
PIECES = 4
NT = (((1,), (1,)), ((), ()))


def cost(flops, moved):
    return pl.CostEstimate(flops=int(flops), bytes_accessed=int(moved), transcendentals=0)


def dispatch_kernel(groups, cap, tok_ref, gain_ref, ids_ref, buf_ref, normed_ref, dest_ref):
    step = pl.program_id(0)
    count = tok_ref.shape[0]

    @pl.when(step == 0)
    def _():
        values = tok_ref[...].astype(jnp.float32)
        scale = lax.rsqrt(jnp.mean(values * values, axis=1, keepdims=True) + EPS)
        normed_ref[...] = (values * scale * gain_ref[...]).astype(jnp.bfloat16)
        ids = ids_ref[...]
        expert = lax.broadcasted_iota(jnp.int32, (groups, count), 0)
        hot = [jnp.where(ids[k : k + 1, :] == expert, 1.0, 0.0) for k in range(2)]
        row = lax.broadcasted_iota(jnp.int32, (count, count), 0)
        col = lax.broadcasted_iota(jnp.int32, (count, count), 1)
        earlier = jnp.where(row < col, 1.0, 0.0).astype(jnp.bfloat16)
        before = jnp.dot((hot[0] + hot[1]).astype(jnp.bfloat16), earlier, preferred_element_type=jnp.float32)
        slots = [jnp.sum(before * h, axis=0, keepdims=True).astype(jnp.int32) for h in hot]
        dest_ref[...] = jnp.concatenate(
            [ids[k : k + 1, :] * cap + slots[k] for k in range(2)] + [jnp.zeros((6, count), jnp.int32)], axis=0
        )

    rows = buf_ref.shape[0]
    place = step * rows + lax.broadcasted_iota(jnp.int32, (rows, count), 0)
    chosen = (place == dest_ref[0:1, :]) | (place == dest_ref[1:2, :])
    pick = jnp.where(chosen, 1.0, 0.0).astype(jnp.bfloat16)
    buf_ref[...] = jnp.dot(pick, normed_ref[...], preferred_element_type=jnp.float32).astype(jnp.bfloat16)


def dispatch(tokens, gain, ids_t, groups, cap):
    count, width = tokens.shape
    total, steps = groups * cap, 4
    return pl.pallas_call(
        functools.partial(dispatch_kernel, groups, cap),
        grid=(steps,),
        in_specs=[
            pl.BlockSpec((count, width), lambda i: (0, 0)),
            pl.BlockSpec((1, width), lambda i: (0, 0)),
            pl.BlockSpec((2, count), lambda i: (0, 0)),
        ],
        out_specs=[
            pl.BlockSpec((total // steps, width), lambda i: (i, 0)),
            pl.BlockSpec((count, width), lambda i: (0, 0)),
            pl.BlockSpec((8, count), lambda i: (0, 0)),
        ],
        out_shape=[
            jax.ShapeDtypeStruct((total, width), jnp.bfloat16),
            jax.ShapeDtypeStruct((count, width), jnp.bfloat16),
            jax.ShapeDtypeStruct((8, count), jnp.int32),
        ],
        cost_estimate=cost(2 * total * count * width, 8 * total * width),
        name="dispatch",
    )(tokens, gain.reshape(1, width), ids_t)


def weigh_kernel(dest_ref, gates_ref, hi_ref, lo_ref):
    count, total = hi_ref.shape
    dest = dest_ref[...].astype(jnp.float32).T
    gates = jnp.concatenate([gates_ref[...], jnp.zeros((6, count), jnp.float32)], axis=0).T
    place = lax.broadcasted_iota(jnp.int32, (count, total), 1).astype(jnp.float32)
    weight = sum(jnp.where(place == dest[:, k : k + 1], gates[:, k : k + 1], 0.0) for k in range(2))
    hi = weight.astype(jnp.bfloat16)
    hi_ref[...] = hi
    lo_ref[...] = (weight - hi.astype(jnp.float32)).astype(jnp.bfloat16)


def weigh(dest, gates_t, total):
    count = gates_t.shape[1]
    shape = jax.ShapeDtypeStruct((count, total), jnp.bfloat16)
    return pl.pallas_call(
        weigh_kernel,
        out_shape=[shape, shape],
        cost_estimate=cost(1e9, 4 * count * total),
        name="weigh",
    )(dest, gates_t)


def hidden_kernel(rows_ref, gate_ref, up_ref, out_ref):
    rows = rows_ref[...]
    gate = lax.dot_general(rows, gate_ref[...], NT, preferred_element_type=jnp.float32)
    upper = lax.dot_general(rows, up_ref[...], NT, preferred_element_type=jnp.float32)
    out_ref[...] = (jax.nn.silu(gate) * upper).astype(jnp.bfloat16)


def hidden_units(rows, both):
    total, width = rows.shape
    units = both.shape[0]
    block = 256
    return pl.pallas_call(
        hidden_kernel,
        grid=(units // block,),
        in_specs=[
            pl.BlockSpec((total, width), lambda i: (0, 0)),
            pl.BlockSpec((block, width), lambda i: (i, 0)),
            pl.BlockSpec((block, width), lambda i: (i, 1)),
        ],
        out_specs=pl.BlockSpec((total, block), lambda i: (0, i)),
        out_shape=jax.ShapeDtypeStruct((total, units), jnp.bfloat16),
        cost_estimate=cost(4 * total * width * units, 2 * total * width + 4 * units * width + 2 * total * units),
        name="hidden_units",
    )(rows, both, both)


def down_kernel(hidden_ref, down_ref, out_ref):
    out_ref[...] = jnp.dot(hidden_ref[...], down_ref[...], preferred_element_type=jnp.float32).astype(jnp.bfloat16)


def down_piece(hidden, down, at, pieces):
    total, units = hidden.shape
    wide = down.shape[1] // pieces
    return pl.pallas_call(
        down_kernel,
        grid=(2,),
        in_specs=[
            pl.BlockSpec((total // 2, units), lambda i: (i, 0)),
            pl.BlockSpec((units, wide), lambda i: (0, at)),
        ],
        out_specs=pl.BlockSpec((total // 2, wide), lambda i: (i, 0)),
        out_shape=jax.ShapeDtypeStruct((total, wide), jnp.bfloat16),
        cost_estimate=cost(2 * total * wide * units, 2 * total * units + 2 * units * wide + 2 * total * wide),
        name=f"down_{at}",
    )(hidden, down)


def side_kernel(normed_ref, vector_ref, both_ref, down_ref, out_ref):
    normed = normed_ref[...]
    half = both_ref.shape[1] // 2
    both = jnp.dot(normed, both_ref[...], preferred_element_type=jnp.float32)
    hidden = (jax.nn.silu(both[:, :half]) * both[:, half:]).astype(jnp.bfloat16)
    mix = jax.nn.sigmoid(jnp.sum(normed.astype(jnp.float32) * vector_ref[...], axis=1, keepdims=True))
    out_ref[...] = mix * jnp.dot(hidden, down_ref[...], preferred_element_type=jnp.float32)


def side_branch(normed, vector, both, down):
    count, width = normed.shape
    return pl.pallas_call(
        side_kernel,
        out_shape=jax.ShapeDtypeStruct((count, width), jnp.float32),
        cost_estimate=cost(2 * count * width * 768, 4e6),
        name="side_branch",
    )(normed, vector.reshape(1, width), both, down)


def combine_kernel(back_ref, hi_ref, lo_ref, side_ref, *rest):
    back = back_ref[...]
    total = jnp.dot(hi_ref[...], back, preferred_element_type=jnp.float32)
    total += jnp.dot(lo_ref[...], back, preferred_element_type=jnp.float32)
    rest[-1][...] = (total + side_ref[...]).astype(jnp.bfloat16)


def combine_piece(back, hi, lo, side, held, at):
    total, wide = back.shape
    count, width = side.shape
    more = [] if held is None else [held]
    return pl.pallas_call(
        combine_kernel,
        grid=(1,),
        in_specs=[
            pl.BlockSpec((total, wide), lambda i: (0, 0)),
            pl.BlockSpec((count, total), lambda i: (0, 0)),
            pl.BlockSpec((count, total), lambda i: (0, 0)),
            pl.BlockSpec((count, wide), lambda i: (0, at)),
        ]
        + [pl.BlockSpec(memory_space=pl.ANY)] * len(more),
        out_specs=pl.BlockSpec((count, wide), lambda i: (0, at)),
        out_shape=jax.ShapeDtypeStruct((count, width), jnp.bfloat16),
        input_output_aliases={4: 0} if more else {},
        cost_estimate=cost(4 * count * total * wide, 2 * total * wide + 4 * count * total + 6 * count * wide),
        name=f"combine_{at}",
    )(back, hi, lo, side, *more)


def dense_weights(dense_gate, dense_up, dense_down):
    ep, tp = lax.axis_size(EP), lax.axis_size("tp")
    t = lax.axis_index("tp")
    deep, fs = dense_gate.shape
    wide = dense_down.shape[1]
    r, q = deep // tp, fs // tp
    both = jnp.concatenate(
        [lax.dynamic_slice_in_dim(a, t * r, r, 0) for a in (dense_gate, dense_up)], axis=1
    )
    own = lax.dynamic_slice_in_dim(dense_down, t * q, q, 0).reshape(-1, 2 * fs)
    mine = jnp.concatenate([both, own, jnp.zeros((16 - r - len(own), 2 * fs), both.dtype)], axis=0)
    near = lax.all_to_all(jnp.broadcast_to(mine[None], (ep, *mine.shape)), EP, split_axis=0, concat_axis=0, tiled=True)
    far = lax.all_gather(near.reshape(-1, 2 * fs), "tp", axis=0, tiled=True).reshape(tp, ep, 16, 2 * fs)
    whole = far[:, :, :r].transpose(1, 0, 2, 3).reshape(ep * deep, 2 * fs)
    down = far[:, :, r : r + len(own)].reshape(tp, ep, q, wide).transpose(0, 2, 1, 3).reshape(fs, ep * wide)
    return whole, down


def on_device(
    tokens, norm_gain, expert_ids, gate_weights, w_gate, w_up, w_down, dense_gate, dense_up, dense_down, mix_vector
):
    count, topk = expert_ids.shape
    width = tokens.shape[1]
    groups = lax.axis_size(EP)
    cap = 2 * count * topk // groups
    turned = [w[0].T for w in (w_gate, w_up, w_down)]
    both = lax.all_gather(jnp.concatenate(turned[:2], axis=1), "tp", axis=0, tiled=True)
    down = lax.all_gather(turned[2], "tp", axis=0, tiled=True)
    buffer, normed, dest = dispatch(tokens, norm_gain, expert_ids.T, groups, cap)
    arrived = lax.all_to_all(buffer.reshape(groups, cap, width), EP, split_axis=0, concat_axis=0, tiled=True)
    hi, lo = weigh(dest, gate_weights.T, groups * cap)
    side = side_branch(normed, mix_vector, *dense_weights(dense_gate, dense_up, dense_down))
    hidden = hidden_units(arrived.reshape(groups * cap, width), both)
    mixed = None
    for at in range(PIECES):
        piece = down_piece(hidden, down, at, PIECES)
        back = lax.all_to_all(piece.reshape(groups, cap, -1), EP, split_axis=0, concat_axis=0, tiled=True)
        mixed = combine_piece(back.reshape(groups * cap, -1), hi, lo, side, mixed, at)
    return mixed


def solution(mesh):
    torus = Mesh(mesh.devices.reshape(4, 4, mesh.shape["tp"]), ("ep_0", "ep_1", "tp"))
    return jax.shard_map(
        on_device,
        mesh=torus,
        in_specs=(
            P(EP_TP, None),
            P(),
            P(EP_TP, None),
            P(EP_TP, None),
            P(EP, None, "tp"),
            P(EP, None, "tp"),
            P(EP, None, "tp"),
            P(EP, None),
            P(EP, None),
            P(None, EP),
            P(),
        ),
        out_specs=P(EP_TP, None),
        check_vma=False,
    )
```

time: 239 us -> 219 us (0.916)
  blocking collectives: 75.2 us -> 0 us
  Pallas kernels: 0 us -> 53.6 us
  matrix products: 37 us -> 0 us
  waiting for transfers between devices: 67.9 us -> 103 us
  starting transfers between devices: 16.6 us -> 36 us
  local copies, waits for them, and re-layouts: 23.7 us -> 10.6 us
  other arithmetic: 4.93 us -> 2.04 us
    all_gather x1 -> x0, blocking collectives: 75.2 us -> none  [whole_of(): nearer = lax.all_gather(x, axes[-1], axis=dim, tiled=True)]
    pallas_call x0 -> x12, Pallas kernels: none -> 53.6 us  [the longest x4 15.3 us: down_piece(): pl.pallas_call(down_kernel, grid=(2,), in_specs=[pl.BlockSpec((total // 2...]
    dot_general x5 -> x0, matrix products: 37 us -> none  [the longest x1 15.5 us: on_device(): lax.dot_general(hidden, pieces[2][0], (((1,), (1,)), ((), ())), preferred...]
    all_to_all x2 -> x6, waiting for transfers between devices: 58.4 us -> 92.9 us  [the longest x1 55.2 us: on_device(): lax.all_to_all(buffer.reshape(groups, cap, width), EP, split_axis=0, conc...]
    all_to_all x2 -> x6, starting transfers between devices: 16.6 us -> 35.9 us  [the longest x4 22.7 us: on_device(): lax.all_to_all(piece.reshape(groups, cap, -1), EP, split_axis=0, concat_a...]
    scatter x1 -> x0, local copies, waits for them, and re-layouts: 12.8 us -> none  [on_device(): jnp.zeros((groups * capacity, width), jnp.bfloat16).at[dest]]
    gather x1 -> x0, local copies, waits for them, and re-layouts: 7.13 us -> none  [on_device(): returned.reshape(groups * capacity, width)[dest]]
    transpose x0 -> x3, local copies, waits for them, and re-layouts: none -> 3.6 us  [the longest x2 3.32 us: dense_weights(): whole = far[:, :, :r].transpose(1, 0, 2, 3).reshape(ep * deep, 2 * fs)]
  transfers between devices with their start and end apart: 5 -> 9, of which waited for: 2 -> 6; matrix products, arithmetic and copies ran while one was open for 25% -> 4% of each run, Pallas kernels for 0% -> 23%
where the time goes in v1:
time: 219 us; the launch traced here: 218 us
  waiting for transfers between devices  103 us (47%)
  Pallas kernels  53.6 us (24%)
  starting transfers between devices  36 us (16%)
  between operations  13.2 us (6%)
  local copies, waits for them, and re-layouts  10.6 us (5%)
    all_to_all x1, waiting for transfers between devices, on_device(): lax.all_to_all(buffer.reshape(groups, cap, width), EP, split_axis=0, conc...  55.2 us
    all_to_all x4, waiting for transfers between devices, on_device(): lax.all_to_all(piece.reshape(groups, cap, -1), EP, split_axis=0, concat_a...  35.7 us
    all_to_all x4, starting transfers between devices, on_device(): lax.all_to_all(piece.reshape(groups, cap, -1), EP, split_axis=0, concat_a...  22.7 us
    pallas_call x4, Pallas kernels, down_piece(): pl.pallas_call(down_kernel, grid=(2,), in_specs=[pl.BlockSpec((total // 2...  15.3 us
    pallas_call x1, Pallas kernels, hidden_units(): pl.pallas_call(hidden_kernel, grid=(units // block,), in_specs=[pl.BlockS...  13.7 us
    pallas_call x4, Pallas kernels, combine_piece(): pl.pallas_call(combine_kernel, grid=(1,), in_specs=[pl.BlockSpec((total,...  12.3 us
    all_gather x1, waiting for transfers between devices, on_device(): down = lax.all_gather(turned[2], 'tp', axis=0, tiled=True)  8.53 us
    all_to_all x1, starting transfers between devices, dense_weights(): lax.all_to_all(jnp.broadcast_to(mine[None], (ep, *mine.shape)), EP, split...  7.48 us
  transfers between devices with their start and end apart: 9, of which 6 were waited for; matrix products, arithmetic and copies ran while one was open for 4% of the time, Pallas kernels for 23%

profile of v1, /device:TPU:2, one launch (start us, length us, event | category | flops | bytes accessed | tf_op | source)
XLA Modules:
  0.0 218.2 jit_solution(6638898110086110170)
XLA Ops:
  6.5 2.0 pad_maximum_fusion
  10.9 7.5 %all-to-all-start.2 = ((bf16[16,16,512]{2,1,0:T(8,128)(2,1)}), bf16[16,16,512]{2,1,0:T(8,128)(2,1)S(1)}, u32[]{:S(2)}, u32[]{:S(2)}) async-start(bf16[16,16,512]{2,1,0:T(8,128)(2,1)} %broadcast_in_dim.10), calls=%async_computation.2 | async-start | bytes 524288 | tf_op jit(solution)/shard_map/all_to_all | solution.py:204
  18.4 5.4 %dispatch.1 = (bf16[1024,2048]{1,0:T(8,128)(2,1)}, bf16[256,2048]{1,0:T(8,128)(2,1)}, s32[8,256]{1,0:T(8,128)}) custom-call(bf16[256,2048]{1,0:T(8,128)(2,1)} %tok_ref.1, f32[1,2048]{1,0:T(1,128)} %bitcast.54, s32[2,256]{1,0:T(2,128)} %bitcast.55), custom_call_target="tpu_custom_call" | custom-call | flops 1073741824 | bytes 16777216 | tf_op jit(solution)/shard_map/dispatch/pallas_call | solution.py:53
  26.5 5.7 %all-to-all-start = ((bf16[16,64,2048]{2,1,0:T(8,128)(2,1)}), bf16[16,64,2048]{2,1,0:T(8,128)(2,1)}, u32[]{:S(2)}, u32[]{:S(2)}) async-start(bf16[16,64,2048]{2,1,0:T(8,128)(2,1)} %bitcast.40), calls=%async_computation | async-start | bytes 8388608 | tf_op jit(solution)/shard_map/all_to_all | solution.py:222
  32.9 55.2 %all-to-all-done = bf16[16,64,2048]{2,1,0:T(8,128)(2,1)} async-done(((bf16[16,64,2048]{2,1,0:T(8,128)(2,1)}), bf16[16,64,2048]{2,1,0:T(8,128)(2,1)}, u32[]{:S(2)}, u32[]{:S(2)}) %all-to-all-start) | async-done | bytes 4194336 | tf_op jit(solution)/shard_map/all_to_all | solution.py:222
  88.2 13.7 %hidden_units.1.hidden_ref = bf16[1024,1024]{1,0:T(8,128)(2,1)} custom-call(bf16[1024,2048]{1,0:T(8,128)(2,1)} %bitcast.3.rows_ref, bf16[1024,4096]{1,0:T(8,128)(2,1)} %all-gather.4.cloned.1.call-done.gate_ref.up_ref, bf16[1024,4096]{1,0:T(8,128)(2,1)} %all-gather.4.cloned.1.call-done.gate_ref.up_ref), custom_call_target="tpu_custom_call" | custom-call | flops 8589934592 | bytes 14680064 | tf_op jit(solution)/shard_map/hidden_units/pallas_call | solution.py:109
  101.9 8.5 %all-gather.6.cloned.1.call-done.down_ref = bf16[1024,2048]{1,0:T(8,128)(2,1)} async-done(((bf16[64,2048]{1,0:T(8,128)(2,1)}), bf16[1024,2048]{1,0:T(8,128)(2,1)}) %all-gather.6.cloned.1.call-update) | async-done | bytes 4194320 | tf_op jit(solution)/shard_map/all_gather | solution.py:220
  110.4 3.8 %down_0.1 = bf16[1024,512]{1,0:T(8,128)(2,1)} custom-call(bf16[1024,1024]{1,0:T(8,128)(2,1)} %hidden_units.1.hidden_ref, bf16[1024,2048]{1,0:T(8,128)(2,1)} %all-gather.6.cloned.1.call-done.down_ref), custom_call_target="tpu_custom_call" | custom-call | flops 1073741824 | bytes 4194304 | tf_op jit(solution)/shard_map/down_0/pallas_call | solution.py:131
  114.2 7.3 %all-to-all-start.5 = ((bf16[16,64,512]{2,1,0:T(8,128)(2,1)}), bf16[16,64,512]{2,1,0:T(8,128)(2,1)S(1)}, u32[]{:S(2)}, u32[]{:S(2)}) async-start(bf16[16,64,512]{2,1,0:T(8,128)(2,1)} %bitcast.39), calls=%async_computation.5 | async-start | bytes 2097152 | tf_op jit(solution)/shard_map/all_to_all | solution.py:229
  121.5 3.8 %down_1.1 = bf16[1024,512]{1,0:T(8,128)(2,1)} custom-call(bf16[1024,1024]{1,0:T(8,128)(2,1)} %hidden_units.1.hidden_ref, bf16[1024,2048]{1,0:T(8,128)(2,1)} %all-gather.6.cloned.1.call-done.down_ref), custom_call_target="tpu_custom_call" | custom-call | flops 1073741824 | bytes 4194304 | tf_op jit(solution)/shard_map/down_1/pallas_call | solution.py:131
  125.3 12.4 %all-to-all-done.5 = bf16[16,64,512]{2,1,0:T(8,128)(2,1)S(1)} async-done(((bf16[16,64,512]{2,1,0:T(8,128)(2,1)}), bf16[16,64,512]{2,1,0:T(8,128)(2,1)S(1)}, u32[]{:S(2)}, u32[]{:S(2)}) %all-to-all-start.5) | async-done | bytes 1048608 | tf_op jit(solution)/shard_map/all_to_all | solution.py:229
  137.7 5.2 %all-to-all-start.4 = ((bf16[16,64,512]{2,1,0:T(8,128)(2,1)}), bf16[16,64,512]{2,1,0:T(8,128)(2,1)S(1)}, u32[]{:S(2)}, u32[]{:S(2)}) async-start(bf16[16,64,512]{2,1,0:T(8,128)(2,1)} %bitcast.38), calls=%async_computation.4 | async-start | bytes 2097152 | tf_op jit(solution)/shard_map/all_to_all | solution.py:229
  142.9 3.9 %down_2.1 = bf16[1024,512]{1,0:T(8,128)(2,1)} custom-call(bf16[1024,1024]{1,0:T(8,128)(2,1)} %hidden_units.1.hidden_ref, bf16[1024,2048]{1,0:T(8,128)(2,1)} %all-gather.6.cloned.1.call-done.down_ref), custom_call_target="tpu_custom_call" | custom-call | flops 1073741824 | bytes 4194304 | tf_op jit(solution)/shard_map/down_2/pallas_call | solution.py:131
  146.7 12.0 %all-to-all-done.4 = bf16[16,64,512]{2,1,0:T(8,128)(2,1)S(1)} async-done(((bf16[16,64,512]{2,1,0:T(8,128)(2,1)}), bf16[16,64,512]{2,1,0:T(8,128)(2,1)S(1)}, u32[]{:S(2)}, u32[]{:S(2)}) %all-to-all-start.4) | async-done | bytes 1048608 | tf_op jit(solution)/shard_map/all_to_all | solution.py:229
  158.7 5.4 %all-to-all-start.3 = ((bf16[16,64,512]{2,1,0:T(8,128)(2,1)}), bf16[16,64,512]{2,1,0:T(8,128)(2,1)S(1)}, u32[]{:S(2)}, u32[]{:S(2)}) async-start(bf16[16,64,512]{2,1,0:T(8,128)(2,1)} %bitcast.37), calls=%async_computation.3 | async-start | bytes 2097152 | tf_op jit(solution)/shard_map/all_to_all | solution.py:229
  164.1 3.8 %down_3.1 = bf16[1024,512]{1,0:T(8,128)(2,1)} custom-call(bf16[1024,1024]{1,0:T(8,128)(2,1)} %hidden_units.1.hidden_ref, bf16[1024,2048]{1,0:T(8,128)(2,1)} %all-gather.6.cloned.1.call-done.down_ref), custom_call_target="tpu_custom_call" | custom-call | flops 1073741824 | bytes 4194304 | tf_op jit(solution)/shard_map/down_3/pallas_call | solution.py:131
  167.9 11.3 %all-to-all-done.3 = bf16[16,64,512]{2,1,0:T(8,128)(2,1)S(1)} async-done(((bf16[16,64,512]{2,1,0:T(8,128)(2,1)}), bf16[16,64,512]{2,1,0:T(8,128)(2,1)S(1)}, u32[]{:S(2)}, u32[]{:S(2)}) %all-to-all-start.3) | async-done | bytes 1048608 | tf_op jit(solution)/shard_map/all_to_all | solution.py:229
  179.3 4.8 %all-to-all-start.1 = ((bf16[16,64,512]{2,1,0:T(8,128)(2,1)}), bf16[16,64,512]{2,1,0:T(8,128)(2,1)S(1)}, u32[]{:S(2)}, u32[]{:S(2)}) async-start(bf16[16,64,512]{2,1,0:T(8,128)(2,1)} %bitcast.36), calls=%async_computation.1 | async-start | bytes 2097152 | tf_op jit(solution)/shard_map/all_to_all | solution.py:229
  184.1 2.3 %weigh.1 = (bf16[256,1024]{1,0:T(8,128)(2,1)}, bf16[256,1024]{1,0:T(8,128)(2,1)}) custom-call(s32[8,256]{1,0:T(8,128)} %get-tuple-element.11.dest_ref, f32[2,256]{1,0:T(2,128)} %bitcast.56), custom_call_target="tpu_custom_call" | custom-call | flops 1000000000 | bytes 1048576 | tf_op jit(solution)/shard_map/weigh/pallas_call | solution.py:90
  193.7 4.6 %side_branch.1.side_ref = f32[256,2048]{1,0:T(8,128)} custom-call(bf16[256,2048]{1,0:T(8,128)(2,1)} %get-tuple-element.14.normed_ref, f32[1,2048]{1,0:T(1,128)} %bitcast.53, bf16[2048,512]{1,0:T(8,128)(2,1)} %bitcast.34, bf16[256,2048]{1,0:T(8,128)(2,1)} %bitcast.46), custom_call_target="tpu_custom_call" | custom-call | flops 805306368 | bytes 4000000 | tf_op jit(solution)/shard_map/side_branch/pallas_call | solution.py:156
  198.3 3.1 %combine_0.1.rest_0_ = bf16[256,2048]{1,0:T(8,128)(2,1)} custom-call(bf16[1024,512]{1,0:T(8,128)(2,1)} %bitcast.35, bf16[256,1024]{1,0:T(8,128)(2,1)} %get-tuple-element.12.hi_ref, bf16[256,1024]{1,0:T(8,128)(2,1)} %get-tuple-element.13.lo_ref, f32[256,2048]{1,0:T(8,128)} %side_branch.1.side_ref), custom_call_target="tpu_custom_call" | custom-call | flops 536870912 | bytes 2883584 | tf_op jit(solution)/shard_map/combine_0/pallas_call | solution.py:175
  201.4 3.1 %combine_1.1.rest_0_ = bf16[256,2048]{1,0:T(8,128)(2,1)} custom-call(bf16[1024,512]{1,0:T(8,128)(2,1)} %bitcast.43, bf16[256,1024]{1,0:T(8,128)(2,1)} %get-tuple-element.12.hi_ref, bf16[256,1024]{1,0:T(8,128)(2,1)} %get-tuple-element.13.lo_ref, f32[256,2048]{1,0:T(8,128)} %side_branch.1.side_ref, ...), custom_call_target="tpu_custom_call", output_to_operand_aliasing={{}: (4, {})} | custom-call | flops 536870912 | bytes 2883584 | tf_op jit(solution)/shard_map/combine_1/pallas_call | solution.py:175
  204.5 3.1 %combine_2.1.rest_0_ = bf16[256,2048]{1,0:T(8,128)(2,1)} custom-call(bf16[1024,512]{1,0:T(8,128)(2,1)} %bitcast.44, bf16[256,1024]{1,0:T(8,128)(2,1)} %get-tuple-element.12.hi_ref, bf16[256,1024]{1,0:T(8,128)(2,1)} %get-tuple-element.13.lo_ref, f32[256,2048]{1,0:T(8,128)} %side_branch.1.side_ref, ...), custom_call_target="tpu_custom_call", output_to_operand_aliasing={{}: (4, {})} | custom-call | flops 536870912 | bytes 2883584 | tf_op jit(solution)/shard_map/combine_2/pallas_call | solution.py:175
  208.6 3.1 %combine_3.1 = bf16[256,2048]{1,0:T(8,128)(2,1)} custom-call(bf16[1024,512]{1,0:T(8,128)(2,1)} %bitcast.45, bf16[256,1024]{1,0:T(8,128)(2,1)} %get-tuple-element.12.hi_ref, bf16[256,1024]{1,0:T(8,128)(2,1)} %get-tuple-element.13.lo_ref, f32[256,2048]{1,0:T(8,128)} %side_branch.1.side_ref, ...), custom_call_target="tpu_custom_call", output_to_operand_aliasing={{}: (4, {})} | custom-call | flops 536870912 | bytes 2883584 | tf_op jit(solution)/shard_map/combine_3/pallas_call | solution.py:175
  (35 shorter events, 14.1 us)
Async XLA Ops:
  6.5 2.8 %copy-start = (bf16[256,128]{1,0:T(8,128)(2,1)S(1)}, bf16[256,128]{1,0:T(8,128)(2,1)}, u32[]{:S(2)}) copy-start(bf16[256,128]{1,0:T(8,128)(2,1)} %param.20) | copy-start | bytes 196612
  6.5 81.6 %all-gather.4.cloned.1.call-start = ((), (), s32[]{:S(2)}) async-start(), calls=%async_computation.6 | async-start | bytes 8912896 | tf_op jit(solution)/shard_map/all_gather | solution.py:219
  8.5 101.9 %all-gather.6.cloned.1.call-start = ((), (), s32[]{:S(2)}) async-start(), calls=%async_computation.7 | async-start | bytes 4456448 | tf_op jit(solution)/shard_map/all_gather | solution.py:220
  10.9 14.8 %all-to-all-start.2 = ((bf16[16,16,512]{2,1,0:T(8,128)(2,1)}), bf16[16,16,512]{2,1,0:T(8,128)(2,1)S(1)}, u32[]{:S(2)}, u32[]{:S(2)}) async-start(bf16[16,16,512]{2,1,0:T(8,128)(2,1)} %broadcast_in_dim.10), calls=%async_computation.2 | async-start | bytes 524288 | tf_op jit(solution)/shard_map/all_to_all | solution.py:204
  25.8 0.7 copy-start.5
  26.5 61.7 %all-to-all-start = ((bf16[16,64,2048]{2,1,0:T(8,128)(2,1)}), bf16[16,64,2048]{2,1,0:T(8,128)(2,1)}, u32[]{:S(2)}, u32[]{:S(2)}) async-start(bf16[16,64,2048]{2,1,0:T(8,128)(2,1)} %bitcast.40), calls=%async_computation | async-start | bytes 8388608 | tf_op jit(solution)/shard_map/all_to_all | solution.py:222
  32.2 154.2 %all-gather.8.cloned.1.call-start = ((), (), s32[]{:S(2)}) async-start(), calls=%async_computation.8 | async-start | bytes 4456448 | tf_op jit(solution)/shard_map/all_gather | solution.py:205
  114.2 23.5 %all-to-all-start.5 = ((bf16[16,64,512]{2,1,0:T(8,128)(2,1)}), bf16[16,64,512]{2,1,0:T(8,128)(2,1)S(1)}, u32[]{:S(2)}, u32[]{:S(2)}) async-start(bf16[16,64,512]{2,1,0:T(8,128)(2,1)} %bitcast.39), calls=%async_computation.5 | async-start | bytes 2097152 | tf_op jit(solution)/shard_map/all_to_all | solution.py:229
  137.7 9.1 %copy-start.1 = (bf16[16,64,512]{2,1,0:T(8,128)(2,1)}, bf16[16,64,512]{2,1,0:T(8,128)(2,1)S(1)}, u32[]{:S(2)}) copy-start(bf16[16,64,512]{2,1,0:T(8,128)(2,1)S(1)} %all-to-all-done.5) | copy-start | bytes 3145732
  137.7 21.0 %all-to-all-start.4 = ((bf16[16,64,512]{2,1,0:T(8,128)(2,1)}), bf16[16,64,512]{2,1,0:T(8,128)(2,1)S(1)}, u32[]{:S(2)}, u32[]{:S(2)}) async-start(bf16[16,64,512]{2,1,0:T(8,128)(2,1)} %bitcast.38), calls=%async_computation.4 | async-start | bytes 2097152 | tf_op jit(solution)/shard_map/all_to_all | solution.py:229
  158.7 9.2 %copy-start.2 = (bf16[16,64,512]{2,1,0:T(8,128)(2,1)}, bf16[16,64,512]{2,1,0:T(8,128)(2,1)S(1)}, u32[]{:S(2)}) copy-start(bf16[16,64,512]{2,1,0:T(8,128)(2,1)S(1)} %all-to-all-done.4) | copy-start | bytes 3145732
  158.7 20.6 %all-to-all-start.3 = ((bf16[16,64,512]{2,1,0:T(8,128)(2,1)}), bf16[16,64,512]{2,1,0:T(8,128)(2,1)S(1)}, u32[]{:S(2)}, u32[]{:S(2)}) async-start(bf16[16,64,512]{2,1,0:T(8,128)(2,1)} %bitcast.37), calls=%async_computation.3 | async-start | bytes 2097152 | tf_op jit(solution)/shard_map/all_to_all | solution.py:229
  179.3 7.1 %copy-start.3 = (bf16[16,64,512]{2,1,0:T(8,128)(2,1)}, bf16[16,64,512]{2,1,0:T(8,128)(2,1)S(1)}, u32[]{:S(2)}) copy-start(bf16[16,64,512]{2,1,0:T(8,128)(2,1)S(1)} %all-to-all-done.3) | copy-start | bytes 3145732
  179.3 28.3 %all-to-all-start.1 = ((bf16[16,64,512]{2,1,0:T(8,128)(2,1)}), bf16[16,64,512]{2,1,0:T(8,128)(2,1)S(1)}, u32[]{:S(2)}, u32[]{:S(2)}) async-start(bf16[16,64,512]{2,1,0:T(8,128)(2,1)} %bitcast.36), calls=%async_computation.1 | async-start | bytes 2097152 | tf_op jit(solution)/shard_map/all_to_all | solution.py:229
  207.6 1.0 copy-start.4
Sparse Core Ops, SparseCore 0:
  9.2 58.7 all-gather.3
  69.8 40.5 all-gather.5
  112.3 40.4 all-gather.7

commit v2 on v1

v2 whole, which is shorter than its diff:
```python
import functools

import jax
import jax.numpy as jnp
from jax import lax
from jax.experimental import pallas as pl
from jax.experimental.pallas import tpu as pltpu
from jax.sharding import Mesh
from jax.sharding import PartitionSpec as P


EP = ("y", "x")
TP = ("z", "core")
ALL = EP + TP
EPS = 1e-06
NT = (((1,), (1,)), ((), ()))
GROUPS = (
    ((2, 1), (2, 3), (0, 2)),
    ((1, 2), (3, 2), (2, 0)),
    ((2, 2), (1, 1), (3, 3), (1, 3), (3, 1)),
    ((0, 1), (1, 0), (0, 3), (3, 0), (0, 0)),
)
SHIFTS = tuple(s for g in GROUPS for s in g)
MIB = 1 << 20


def cost(flops, moved):
    return pl.CostEstimate(flops=int(flops), bytes_accessed=int(moved), transcendentals=0)


def whole(shape):
    return pl.BlockSpec(shape, lambda *_: (0,) * len(shape))


def bf16(*shape):
    return jax.ShapeDtypeStruct(shape, jnp.bfloat16)


def one_row(a):
    return jnp.concatenate([a[i : i + 1, :] for i in range(a.shape[0])], axis=1)


def dispatch_kernel(
    groups, cap, at_ref, tok_ref, gain_ref, ids_ref, dg_ref, du_ref, dd_ref, buf_ref, normed_ref, place_ref, dest_ref, extra_ref
):
    step = pl.program_id(0)
    count = tok_ref.shape[0]
    nx = 4

    @pl.when(step == 0)
    def _():
        values = tok_ref[...].astype(jnp.float32)
        scale = lax.rsqrt(jnp.mean(values * values, axis=1, keepdims=True) + EPS)
        normed_ref[...] = (values * scale * gain_ref[...]).astype(jnp.bfloat16)
        ids = ids_ref[...]
        expert = lax.broadcasted_iota(jnp.int32, (groups, count), 0)
        hot = [jnp.where(ids[k : k + 1, :] == expert, 1.0, 0.0) for k in range(2)]
        row = lax.broadcasted_iota(jnp.int32, (count, count), 0)
        col = lax.broadcasted_iota(jnp.int32, (count, count), 1)
        earlier = jnp.where(row < col, 1.0, 0.0).astype(jnp.bfloat16)
        before = jnp.dot((hot[0] + hot[1]).astype(jnp.bfloat16), earlier, preferred_element_type=jnp.float32)
        slots = [jnp.sum(before * h, axis=0, keepdims=True).astype(jnp.int32) for h in hot]
        rest = [jnp.zeros((6, count), jnp.int32)]
        dest_ref[...] = jnp.concatenate([ids[k : k + 1, :] * cap + slots[k] for k in range(2)] + rest, axis=0)
        shift = ((ids >> 2) + nx - at_ref[0]) % nx * nx + ((ids & 3) + nx - at_ref[1]) % nx
        near = sum(jnp.where(shift == a * nx + b, k, 0) for k, (a, b) in enumerate(SHIFTS))
        place_ref[...] = jnp.concatenate([near[k : k + 1, :] * cap + slots[k] for k in range(2)] + rest, axis=0)
        fs, part = dd_ref.shape[0], dd_ref.shape[0] // 16
        unit = at_ref[2] * part + lax.broadcasted_iota(jnp.int32, (part, fs), 0)
        own = jnp.where(lax.broadcasted_iota(jnp.int32, (part, fs), 1) == unit, 1.0, 0.0).astype(jnp.bfloat16)
        shares = [lax.dot_general(own, r[...], NT, preferred_element_type=jnp.float32) for r in (dg_ref, du_ref)]
        shares += [jnp.dot(own, dd_ref[...], preferred_element_type=jnp.float32)]
        rows = [one_row(v) for v in shares]
        extra_ref[...] = jnp.concatenate(rows + [jnp.zeros((5, rows[0].shape[1]), jnp.float32)], axis=0).astype(jnp.bfloat16)

    many, _, _ = buf_ref.shape
    place = step * many * cap + lax.broadcasted_iota(jnp.int32, (many * cap, count), 0)
    chosen = (place == dest_ref[0:1, :]) | (place == dest_ref[1:2, :])
    pick = jnp.where(chosen, 1.0, 0.0).astype(jnp.bfloat16)
    rows = jnp.dot(pick, normed_ref[...], preferred_element_type=jnp.float32).astype(jnp.bfloat16)
    for i in range(many):
        buf_ref[i, :cap, :] = rows[i * cap : (i + 1) * cap, :]
        buf_ref[i, cap:, :] = extra_ref[...]


def dispatch(at, tokens, gain, ids_t, dense, groups, cap):
    count, width = tokens.shape
    steps, tall = 4, cap + 8
    return pl.pallas_call(
        functools.partial(dispatch_kernel, groups, cap),
        grid=(steps,),
        in_specs=[pl.BlockSpec(memory_space=pltpu.SMEM)]
        + [whole(a) for a in ((count, width), (1, width), (2, count))]
        + [whole(d.shape) for d in dense],
        out_specs=[
            pl.BlockSpec((groups // steps, tall, width), lambda i: (i, 0, 0)),
            whole((count, width)),
            whole((8, count)),
        ],
        out_shape=[bf16(groups, tall, width), bf16(count, width), jax.ShapeDtypeStruct((8, count), jnp.int32)],
        scratch_shapes=[pltpu.VMEM((8, count), jnp.int32), pltpu.VMEM((8, width), jnp.bfloat16)],
        cost_estimate=cost(2 * groups * cap * count * width, 8 * groups * cap * width),
        name="dispatch",
    )(at, tokens, gain.reshape(1, width), ids_t, *dense)


def weigh_kernel(dest_ref, gates_ref, hi_ref, lo_ref):
    count, total = hi_ref.shape
    dest = dest_ref[...].astype(jnp.float32).T
    gates = jnp.concatenate([gates_ref[...], jnp.zeros((6, count), jnp.float32)], axis=0).T
    place = lax.broadcasted_iota(jnp.int32, (count, total), 1).astype(jnp.float32)
    weight = sum(jnp.where(place == dest[:, k : k + 1], gates[:, k : k + 1], 0.0) for k in range(2))
    hi = weight.astype(jnp.bfloat16)
    hi_ref[...] = hi
    lo_ref[...] = (weight - hi.astype(jnp.float32)).astype(jnp.bfloat16)


def weigh(dest, gates_t, total):
    count = gates_t.shape[1]
    return pl.pallas_call(
        weigh_kernel,
        out_shape=[bf16(count, total)] * 2,
        cost_estimate=cost(2e9, 4 * count * total),
        name="weigh",
    )(dest, gates_t)


def hidden_kernel(rows_ref, gate_ref, up_ref, out_ref):
    groups, cap, width = rows_ref.shape
    part = 4
    for at in range(0, groups, part):
        rows = rows_ref[at : at + part].reshape(part * cap, width)
        gate = lax.dot_general(rows, gate_ref[...], NT, preferred_element_type=jnp.float32)
        upper = lax.dot_general(rows, up_ref[...], NT, preferred_element_type=jnp.float32)
        out_ref[at * cap : (at + part) * cap, :] = (jax.nn.silu(gate) * upper).astype(jnp.bfloat16)


def hidden_units(arrived, weights, cap):
    groups, _, width = arrived.shape
    units, block = weights.shape[0], 256
    total = groups * cap
    return pl.pallas_call(
        hidden_kernel,
        grid=(units // block,),
        in_specs=[
            pl.BlockSpec((groups, cap, width), lambda i: (0, 0, 0)),
            pl.BlockSpec((block, width), lambda i: (i, 0)),
            pl.BlockSpec((block, width), lambda i: (i, 1)),
        ],
        out_specs=pl.BlockSpec((total, block), lambda i: (0, i)),
        out_shape=bf16(total, units),
        cost_estimate=cost(4 * total * width * units, 2 * total * width + 4 * units * width + 2 * total * units),
        name="hidden_units",
    )(arrived, weights, weights)


def down_kernel(many, at_ref, *refs):
    rows, down_ref, outs = refs[:many], refs[many], refs[many + 1 :]
    cap = outs[0].shape[0]
    hidden = jnp.concatenate([r[...] for r in rows], axis=0)
    result = jnp.dot(hidden, down_ref[...], preferred_element_type=jnp.float32).astype(jnp.bfloat16)
    for i, out in enumerate(outs):
        out[...] = result[i * cap : (i + 1) * cap, :]


def down_group(source, hidden, weights, cap, start, many):
    units, width = weights.shape[0], weights.shape[1] // 3
    wide = 512
    skip = 2 * width // wide
    return pl.pallas_call(
        functools.partial(down_kernel, many),
        grid_spec=pltpu.PrefetchScalarGridSpec(
            num_scalar_prefetch=1,
            grid=(width // wide,),
            in_specs=[pl.BlockSpec((cap, units), lambda i, at, k=k: (at[start + k], 0)) for k in range(many)]
            + [pl.BlockSpec((units, wide), lambda i, at: (0, skip + i))],
            out_specs=[pl.BlockSpec((cap, wide), lambda i, at: (0, i))] * many,
        ),
        out_shape=[bf16(cap, width)] * many,
        compiler_params=pltpu.CompilerParams(vmem_limit_bytes=54 * MIB),
        cost_estimate=cost(2 * many * cap * width * units, 2 * units * width + 4 * many * cap * width),
    )(source, *[hidden] * many, weights)


def side_kernel(normed_ref, vector_ref, dense_ref, out_ref):
    normed = normed_ref[...]
    gate, up, down = (jnp.concatenate([dense_ref[t, k] for t in range(dense_ref.shape[0])], axis=0) for k in range(3))
    dense_g = lax.dot_general(normed, gate, NT, preferred_element_type=jnp.float32)
    dense_u = lax.dot_general(normed, up, NT, preferred_element_type=jnp.float32)
    hidden = (jax.nn.silu(dense_g) * dense_u).astype(jnp.bfloat16)
    mix = jax.nn.sigmoid(jnp.sum(normed.astype(jnp.float32) * vector_ref[...], axis=1, keepdims=True))
    out_ref[...] = mix * jnp.dot(hidden, down, preferred_element_type=jnp.float32)


def side_branch(normed, vector, dense):
    count, width = normed.shape
    return pl.pallas_call(
        side_kernel,
        out_shape=jax.ShapeDtypeStruct((count, width), jnp.float32),
        compiler_params=pltpu.CompilerParams(vmem_limit_bytes=24 * MIB),
        cost_estimate=cost(2 * count * width * 768, 4e6),
        name="side_branch",
    )(normed, vector.reshape(1, width), dense)


def combine_kernel(start, many, *refs):
    backs, (hi_ref, lo_ref, add_ref, out_ref) = refs[:many], refs[many:]
    cap = backs[0].shape[0]
    back = jnp.concatenate([b[...] for b in backs], axis=0)
    at = slice(start * cap, (start + many) * cap)
    total = add_ref[...] + jnp.dot(hi_ref[:, at], back, preferred_element_type=jnp.float32)
    total += jnp.dot(lo_ref[:, at], back, preferred_element_type=jnp.float32)
    out_ref[...] = total.astype(out_ref.dtype)


def combine(backs, hi, lo, add, start, dtype):
    many, (cap, width) = len(backs), backs[0].shape
    count, total = hi.shape
    wide = 1024
    column = lambda i: (0, i)
    return pl.pallas_call(
        functools.partial(combine_kernel, start, many),
        grid=(width // wide,),
        in_specs=[pl.BlockSpec((cap, wide), column)] * many
        + [whole((count, total))] * 2
        + [pl.BlockSpec((count, wide), column)],
        out_specs=pl.BlockSpec((count, wide), column),
        out_shape=jax.ShapeDtypeStruct((count, width), dtype),
        compiler_params=pltpu.CompilerParams(vmem_limit_bytes=20 * MIB),
        cost_estimate=cost(4 * count * many * cap * width, 2 * many * cap * width + 8 * count * width),
    )(*backs, hi, lo, add)


def shifted(a, shift):
    if shift == (0, 0):
        return a
    dy, dx = shift
    ny, nx = lax.axis_size("y"), lax.axis_size("x")
    pairs = [(y * nx + x, (y + dy) % ny * nx + (x + dx) % nx) for y in range(ny) for x in range(nx)]
    return lax.ppermute(a, EP, pairs)


def on_device(
    tokens, norm_gain, expert_ids, gate_weights, w_gate, w_up, w_down, dense_gate, dense_up, dense_down, mix_vector
):
    count, topk = expert_ids.shape
    width = tokens.shape[1]
    groups, tp = lax.axis_size(EP), lax.axis_size(TP)
    ny, nx = lax.axis_size("y"), lax.axis_size("x")
    y, x = lax.axis_index("y"), lax.axis_index("x")
    cap = 2 * count * topk // groups
    weights = jnp.concatenate([w[0].T for w in (w_gate, w_up, w_down)], axis=1)
    weights = lax.all_gather(weights, TP, axis=0, tiled=True)

    at = jnp.stack([y, x, lax.axis_index(TP)]).astype(jnp.int32)
    dense = (dense_gate, dense_up, dense_down)
    buffer, normed, dest = dispatch(at, tokens, norm_gain, expert_ids.T, dense, groups, cap)
    arrived = lax.all_to_all(buffer, EP, split_axis=0, concat_axis=0, tiled=True)
    hi, lo = weigh(dest, gate_weights.T, groups * cap)
    part = dense_down.shape[0] // tp
    dense = arrived[:, cap : cap + 3].reshape(groups, 3, part, -1).transpose(1, 2, 0, 3)
    dense = lax.all_gather(dense.reshape(3 * part, width), TP, axis=0, tiled=True)
    dense = dense.reshape(tp, 3, part, width)
    hidden = hidden_units(arrived, weights, cap)
    down_y, down_x = (jnp.array(v, jnp.int32) for v in zip(*SHIFTS))
    source = ((y - down_y) % ny * nx + (x - down_x) % nx).astype(jnp.int32)
    backs = []
    for group in GROUPS:
        results = down_group(source, hidden, weights, cap, len(backs), len(group))
        backs += [shifted(a, (-s[0] % ny, -s[1] % nx)) for a, s in zip(results, group)]
    side = side_branch(normed, mix_vector, dense)
    cut = groups - len(GROUPS[-1])
    part = combine(backs[:cut], hi, lo, side, 0, jnp.float32)
    return combine(backs[cut:], hi, lo, part, cut, jnp.bfloat16)


def solution(mesh):
    tp = mesh.shape["tp"]
    torus = Mesh(mesh.devices.reshape(4, 4, tp // 2, 2), ALL)
    return jax.shard_map(
        on_device,
        mesh=torus,
        in_specs=(
            P(ALL, None),
            P(),
            P(ALL, None),
            P(ALL, None),
            P(EP, None, TP),
            P(EP, None, TP),
            P(EP, None, TP),
            P(EP, None),
            P(EP, None),
            P(None, EP),
            P(),
        ),
        out_specs=P(ALL, None),
        check_vma=False,
    )
```

time: 219 us -> 183 us (0.84)
  the two profiles are of different devices: /device:TPU:2 before, /device:TPU:1 now
where the time goes in v2:
time: 183 us; the launch traced here: 182 us
  blocking collectives  63.1 us (34%)
  Pallas kernels  51.1 us (28%)
  starting transfers between devices  24.8 us (14%)
  waiting for transfers between devices  20.6 us (11%)
  between operations  13.6 us (7%)
  local copies, waits for them, and re-layouts  5.92 us (3%)
  other arithmetic  3.23 us (2%)
    all_to_all x1, blocking collectives, on_device(): lax.all_to_all(buffer, EP, split_axis=0, concat_axis=0, tiled=True)  63.1 us
    ppermute x15, starting transfers between devices, shifted(): return lax.ppermute(a, EP, pairs)  24.7 us
    pallas_call x4, Pallas kernels, down_group(): pl.pallas_call(functools.partial(down_kernel, many), grid_spec=pltpu.Pref...  22.4 us
    pallas_call x1, Pallas kernels, hidden_units(): pl.pallas_call(hidden_kernel, grid=(units // block,), in_specs=[pl.BlockS...  13.3 us
    ppermute x15, waiting for transfers between devices, shifted(): return lax.ppermute(a, EP, pairs)  13.2 us
    all_gather x1, waiting for transfers between devices, on_device(): weights = lax.all_gather(weights, TP, axis=0, tiled=True)  7.36 us
    pallas_call x2, Pallas kernels, combine(): pl.pallas_call(functools.partial(combine_kernel, start, many), grid=(widt...  6.6 us
    unnamed x25, local copies, waits for them, and re-layouts  5.55 us
  transfers between devices with their start and end apart: 17, of which 6 were waited for; matrix products, arithmetic and copies ran while one was open for 1% of the time, Pallas kernels for 26%

profile of v2, /device:TPU:1, one launch (start us, length us, event | category | flops | bytes accessed | tf_op | source)
XLA Modules:
  0.0 182.2 jit_solution(8430829189296994652)
XLA Ops:
  6.5 2.0 %pad_maximum_fusion = bf16[64,6144]{1,0:T(8,128)(2,1)} fusion(bf16[64,2048]{1,0:T(8,128)(2,1)} %bitcast.29, bf16[64,2048]{1,0:T(8,128)(2,1)} %bitcast.30, bf16[64,2048]{1,0:T(8,128)(2,1)} %bitcast.31), kind=kLoop, calls=%fused_computation | loop fusion | flops 2359296 | bytes 1572864 | tf_op jit(solution)/shard_map/concatenate | solution.py:252
  9.3 5.4 %dispatch.1 = (bf16[16,72,2048]{2,1,0:T(8,128)(2,1)}, bf16[256,2048]{1,0:T(8,128)(2,1)}, s32[8,256]{1,0:T(8,128)}) custom-call(s32[3]{0:T(128)} %pad_add_fusion.at_ref, bf16[256,2048]{1,0:T(8,128)(2,1)} %tok_ref.1, f32[1,2048]{1,0:T(1,128)} %bitcast.32, s32[2,256]{1,0:T(2,128)} %bitcast.33, bf16[128,256]{1,0:T(8,128)(2,1)} %dg_ref.1, ...), custom_call_target="tpu_custom_call" | custom-call | flops 1073741824 | bytes 16777216 | tf_op jit(solution)/shard_map/dispatch/pallas_call | solution.py:89
  14.7 63.1 %all_to_all.5.rows_ref = bf16[16,72,2048]{2,1,0:T(8,128)(2,1)S(1)} all-to-all(bf16[16,72,2048]{2,1,0:T(8,128)(2,1)} %get-tuple-element.26), channel_id=1, replica_groups=mesh['y'=4,'x'=4,'z'=8,'core'=2] {'y','x'}, dimensions={0} | all-to-all | bytes 9437184 | tf_op jit(solution)/shard_map/all_to_all | solution.py:258
  77.8 2.1 %copy-done.8 = bf16[16,72,2048]{2,1,0:T(8,128)(2,1)} copy-done((bf16[16,72,2048]{2,1,0:T(8,128)(2,1)}, bf16[16,72,2048]{2,1,0:T(8,128)(2,1)S(1)}, u32[]{:S(2)}) %copy-start.8) | copy-done | bytes 4718616
  81.6 7.4 %all-gather.3.cloned.1.call-done.gate_ref.up_ref.refs_5_.refs_3_ = bf16[1024,6144]{1,0:T(8,128)(2,1)} async-done(((bf16[64,6144]{1,0:T(8,128)(2,1)}), bf16[1024,6144]{1,0:T(8,128)(2,1)}) %all-gather.3.cloned.1.call-update) | async-done | bytes 12582928 | tf_op jit(solution)/shard_map/all_gather | solution.py:253
  89.0 13.3 %hidden_units.1.refs_0_.refs_1_.refs_2_.refs_3_.refs_4_ = bf16[1024,1024]{1,0:T(8,128)(2,1)} custom-call(bf16[16,72,2048]{2,1,0:T(8,128)(2,1)} %copy-done.8, bf16[1024,6144]{1,0:T(8,128)(2,1)} %all-gather.3.cloned.1.call-done.gate_ref.up_ref.refs_5_.refs_3_, bf16[1024,6144]{1,0:T(8,128)(2,1)} %all-gather.3.cloned.1.call-done.gate_ref.up_ref.refs_5_.refs_3_), custom_call_target="tpu_custom_call" | custom-call | flops 8589934592 | bytes 14680064 | tf_op jit(solution)/shard_map/hidden_units/pallas_call | solution.py:142
  102.3 5.4 %shard_map.129 = (bf16[64,2048]{1,0:T(8,128)(2,1)}, bf16[64,2048]{1,0:T(8,128)(2,1)}, bf16[64,2048]{1,0:T(8,128)(2,1)}) custom-call(s32[16]{0:T(128)} %fusion.at_ref, bf16[1024,1024]{1,0:T(8,128)(2,1)} %hidden_units.1.refs_0_.refs_1_.refs_2_.refs_3_.refs_4_, bf16[1024,1024]{1,0:T(8,128)(2,1)} %hidden_units.1.refs_0_.refs_1_.refs_2_.refs_3_.refs_4_, ...), custom_call_target="tpu_custom_call" | custom-call | flops 805306368 | bytes 5767168 | tf_op jit(solution)/shard_map/pallas_call | solution.py:170
  107.7 4.9 %collective-permute-start.7 = (bf16[64,2048]{1,0:T(8,128)(2,1)}, bf16[64,2048]{1,0:T(8,128)(2,1)S(1)}, u32[]{:S(2)}, u32[]{:S(2)}) collective-permute-start(bf16[64,2048]{1,0:T(8,128)(2,1)} %get-tuple-element.38), channel_id=1, source_target_pairs={{0,224},{16,240},{32,192},{48,208},{64,32},{80,48},{96,0},{112,16}... | collective-permute-start | bytes 786440 | tf_op jit(solution)/shard_map/ppermute | solution.py:240
  112.6 1.7 collective-permute-start.9
  114.3 5.4 %shard_map.128 = (bf16[64,2048]{1,0:T(8,128)(2,1)}, bf16[64,2048]{1,0:T(8,128)(2,1)}, bf16[64,2048]{1,0:T(8,128)(2,1)}) custom-call(s32[16]{0:T(128)} %fusion.at_ref, bf16[1024,1024]{1,0:T(8,128)(2,1)} %hidden_units.1.refs_0_.refs_1_.refs_2_.refs_3_.refs_4_, bf16[1024,1024]{1,0:T(8,128)(2,1)} %hidden_units.1.refs_0_.refs_1_.refs_2_.refs_3_.refs_4_, ...), custom_call_target="tpu_custom_call" | custom-call | flops 805306368 | bytes 5767168 | tf_op jit(solution)/shard_map/pallas_call | solution.py:170
  119.7 2.3 %collective-permute-start.4 = (bf16[64,2048]{1,0:T(8,128)(2,1)}, bf16[64,2048]{1,0:T(8,128)(2,1)S(1)}, u32[]{:S(2)}, u32[]{:S(2)}) collective-permute-start(bf16[64,2048]{1,0:T(8,128)(2,1)} %get-tuple-element.35), channel_id=1, source_target_pairs={{0,176},{16,128},{32,144},{48,160},{64,240},{80,192},{96,208},{112... | collective-permute-start | bytes 786440 | tf_op jit(solution)/shard_map/ppermute | solution.py:240
  122.1 1.5 collective-permute-start.5
  123.6 5.8 %shard_map.130 = (bf16[64,2048]{1,0:T(8,128)(2,1)}, bf16[64,2048]{1,0:T(8,128)(2,1)}, bf16[64,2048]{1,0:T(8,128)(2,1)}, bf16[64,2048]{1,0:T(8,128)(2,1)}, bf16[64,2048]{1,0:T(8,128)(2,1)}) custom-call(s32[16]{0:T(128)} %fusion.at_ref, bf16[1024,1024]{1,0:T(8,128)(2,1)} %hidden_units.1.refs_0_.refs_1_.refs_2_.refs_3_.refs_4_, ...), custom_call_target="tpu_custom_call" | custom-call | flops 1342177280 | bytes 6815744 | tf_op jit(solution)/shard_map/pallas_call | solution.py:170
  129.4 2.8 %collective-permute-start.6 = (bf16[64,2048]{1,0:T(8,128)(2,1)S(1)}, bf16[64,2048]{1,0:T(8,128)(2,1)S(1)}, u32[]{:S(2)}, u32[]{:S(2)}) collective-permute-start(bf16[64,2048]{1,0:T(8,128)(2,1)S(1)} %copy-done.11), channel_id=1, source_target_pairs={{0,32},{16,48},{32,0},{48,16},{64,96},{80,112},{96,64},{112,80},{1... | collective-permute-start | bytes 786440 | tf_op jit(solution)/shard_map/ppermute | solution.py:240
  133.5 4.9 %collective-permute-done.9.refs_5_ = bf16[64,2048]{1,0:T(8,128)(2,1)S(1)} collective-permute-done((bf16[64,2048]{1,0:T(8,128)(2,1)}, bf16[64,2048]{1,0:T(8,128)(2,1)S(1)}, u32[]{:S(2)}, u32[]{:S(2)}) %collective-permute-start.9) | collective-permute-done | bytes 262176 | tf_op jit(solution)/shard_map/ppermute | solution.py:240
  141.7 5.8 %shard_map.127 = (bf16[64,2048]{1,0:T(8,128)(2,1)}, bf16[64,2048]{1,0:T(8,128)(2,1)}, bf16[64,2048]{1,0:T(8,128)(2,1)}, bf16[64,2048]{1,0:T(8,128)(2,1)}, bf16[64,2048]{1,0:T(8,128)(2,1)}) custom-call(s32[16]{0:T(128)} %fusion.at_ref, bf16[1024,1024]{1,0:T(8,128)(2,1)} %hidden_units.1.refs_0_.refs_1_.refs_2_.refs_3_.refs_4_, ...), custom_call_target="tpu_custom_call" | custom-call | flops 1342177280 | bytes 6815744 | tf_op jit(solution)/shard_map/pallas_call | solution.py:170
  147.5 2.8 %collective-permute-start.14 = (bf16[64,2048]{1,0:T(8,128)(2,1)}, bf16[64,2048]{1,0:T(8,128)(2,1)}, u32[]{:S(2)}, u32[]{:S(2)}) collective-permute-start(bf16[64,2048]{1,0:T(8,128)(2,1)} %get-tuple-element.45), channel_id=1, source_target_pairs={{0,112},{16,64},{32,80},{48,96},{64,176},{80,128},{96,144},{112,16... | collective-permute-start | bytes 786440 | tf_op jit(solution)/shard_map/ppermute | solution.py:240
  151.3 1.9 %collective-permute-done.11.refs_7_ = bf16[64,2048]{1,0:T(8,128)(2,1)S(1)} collective-permute-done((bf16[64,2048]{1,0:T(8,128)(2,1)}, bf16[64,2048]{1,0:T(8,128)(2,1)S(1)}, u32[]{:S(2)}, u32[]{:S(2)}) %collective-permute-start.11) | collective-permute-done | bytes 262176 | tf_op jit(solution)/shard_map/ppermute | solution.py:240
  154.7 2.2 %collective-permute-start.2 = (bf16[64,2048]{1,0:T(8,128)(2,1)}, bf16[64,2048]{1,0:T(8,128)(2,1)}, u32[]{:S(2)}, u32[]{:S(2)}) collective-permute-start(bf16[64,2048]{1,0:T(8,128)(2,1)} %get-tuple-element.29), channel_id=1, source_target_pairs={{0,16},{16,32},{32,48},{48,0},{64,80},{80,96},{96,112},{112,64},{1... | collective-permute-start | bytes 786440 | tf_op jit(solution)/shard_map/ppermute | solution.py:240
  157.0 5.4 %collective-permute-done.13.refs_9_ = bf16[64,2048]{1,0:T(8,128)(2,1)S(1)} collective-permute-done((bf16[64,2048]{1,0:T(8,128)(2,1)}, bf16[64,2048]{1,0:T(8,128)(2,1)S(1)}, u32[]{:S(2)}, u32[]{:S(2)}) %collective-permute-start.13) | collective-permute-done | bytes 262176 | tf_op jit(solution)/shard_map/ppermute | solution.py:240
  163.1 2.3 %weigh.1 = (bf16[256,1024]{1,0:T(8,128)(2,1)}, bf16[256,1024]{1,0:T(8,128)(2,1)}) custom-call(s32[8,256]{1,0:T(8,128)} %get-tuple-element.32.dest_ref, f32[2,256]{1,0:T(2,128)} %bitcast.34), custom_call_target="tpu_custom_call" | custom-call | flops 2000000000 | bytes 1048576 | tf_op jit(solution)/shard_map/weigh/pallas_call | solution.py:120
  165.4 1.9 %copy-done = bf16[768,2048]{1,0:T(8,128)(2,1)S(1)} copy-done((bf16[768,2048]{1,0:T(8,128)(2,1)S(1)}, bf16[768,2048]{1,0:T(8,128)(2,1)}, u32[]{:S(2)}) %copy-start) | copy-done | bytes 3145752
  168.5 3.2 %shard_map.131.refs_7_ = f32[256,2048]{1,0:T(8,128)S(1)} custom-call(bf16[64,2048]{1,0:T(8,128)(2,1)S(1)} %collective-permute-done.4.refs_0_, bf16[64,2048]{1,0:T(8,128)(2,1)S(1)} %collective-permute-done.5.refs_1_, bf16[64,2048]{1,0:T(8,128)(2,1)S(1)} %collective-permute-done.6.refs_2_, bf16[64,2048]{1,0:T(8,128)(2,1)S(1)} %collective-permute-done.7.refs_3_, ...), custom_call_target="tpu_custom_call" | custom-call | flops 1476395008 | bytes 7077888 | tf_op jit(solution)/shard_map/pallas_call | solution.py:221
  172.0 3.4 %shard_map.132 = bf16[256,2048]{1,0:T(8,128)(2,1)} custom-call(bf16[64,2048]{1,0:T(8,128)(2,1)} %collective-permute-done.refs_0_, bf16[64,2048]{1,0:T(8,128)(2,1)} %collective-permute-done.1.refs_1_, bf16[64,2048]{1,0:T(8,128)(2,1)} %collective-permute-done.2.refs_2_, bf16[64,2048]{1,0:T(8,128)(2,1)} %collective-permute-done.3.refs_3_, ...), custom_call_target="tpu_custom_call" | custom-call | flops 671088640 | bytes 5505024 | tf_op jit(solution)/shard_map/pallas_call | solution.py:221
  (54 shorter events, 11.8 us)
Async XLA Ops:
  6.5 82.5 %all-gather.3.cloned.1.call-start = ((), (), s32[]{:S(2)}) async-start(), calls=%async_computation.1 | async-start | bytes 13369344 | tf_op jit(solution)/shard_map/all_gather | solution.py:253
  8.6 156.8 %all-gather.5.cloned.1.call-start = ((), (), s32[]{:S(2)}) async-start(), calls=%async_computation.2 | async-start | bytes 3342336 | tf_op jit(solution)/shard_map/all_gather | solution.py:262
  14.7 66.3 %copy-start.9 = (s32[16]{0:T(128)S(1)}, s32[16]{0:T(128)}, u32[]{:S(2)}) copy-start(s32[16]{0:T(128)} %constant.51) | copy-start | bytes 196
  14.7 66.4 %copy-start.10 = (s32[16]{0:T(128)S(1)}, s32[16]{0:T(128)}, u32[]{:S(2)}) copy-start(s32[16]{0:T(128)} %constant.50) | copy-start | bytes 196
  77.8 2.1 %copy-start.8 = (bf16[16,72,2048]{2,1,0:T(8,128)(2,1)}, bf16[16,72,2048]{2,1,0:T(8,128)(2,1)S(1)}, u32[]{:S(2)}) copy-start(bf16[16,72,2048]{2,1,0:T(8,128)(2,1)S(1)} %all_to_all.5.rows_ref) | copy-start | bytes 14155780
  107.7 21.7 %collective-permute-start.7 = (bf16[64,2048]{1,0:T(8,128)(2,1)}, bf16[64,2048]{1,0:T(8,128)(2,1)S(1)}, u32[]{:S(2)}, u32[]{:S(2)}) collective-permute-start(bf16[64,2048]{1,0:T(8,128)(2,1)} %get-tuple-element.38), channel_id=1, source_target_pairs={{0,224},{16,240},{32,192},{48,208},{64,32},{80,48},{96,0},{112,16}... | collective-permute-start | bytes 786440 | tf_op jit(solution)/shard_map/ppermute | solution.py:240
  112.6 19.6 %collective-permute-start.8 = (bf16[64,2048]{1,0:T(8,128)(2,1)}, bf16[64,2048]{1,0:T(8,128)(2,1)S(1)}, u32[]{:S(2)}, u32[]{:S(2)}) collective-permute-start(bf16[64,2048]{1,0:T(8,128)(2,1)} %get-tuple-element.39), channel_id=1, source_target_pairs={{0,96},{16,112},{32,64},{48,80},{64,160},{80,176},{96,128},{112,14... | collective-permute-start | bytes 786440 | tf_op jit(solution)/shard_map/ppermute | solution.py:240
  112.6 25.9 %collective-permute-start.9 = (bf16[64,2048]{1,0:T(8,128)(2,1)}, bf16[64,2048]{1,0:T(8,128)(2,1)S(1)}, u32[]{:S(2)}, u32[]{:S(2)}) collective-permute-start(bf16[64,2048]{1,0:T(8,128)(2,1)} %get-tuple-element.40), channel_id=1, source_target_pairs={{0,128},{16,144},{32,160},{48,176},{64,192},{80,208},{96,224},{112... | collective-permute-start | bytes 786440 | tf_op jit(solution)/shard_map/ppermute | solution.py:240
  119.7 19.7 %collective-permute-start.4 = (bf16[64,2048]{1,0:T(8,128)(2,1)}, bf16[64,2048]{1,0:T(8,128)(2,1)S(1)}, u32[]{:S(2)}, u32[]{:S(2)}) collective-permute-start(bf16[64,2048]{1,0:T(8,128)(2,1)} %get-tuple-element.35), channel_id=1, source_target_pairs={{0,176},{16,128},{32,144},{48,160},{64,240},{80,192},{96,208},{112... | collective-permute-start | bytes 786440 | tf_op jit(solution)/shard_map/ppermute | solution.py:240
  122.1 7.3 %copy-start.11 = (bf16[64,2048]{1,0:T(8,128)(2,1)S(1)}, bf16[64,2048]{1,0:T(8,128)(2,1)}, u32[]{:S(2)}) copy-start(bf16[64,2048]{1,0:T(8,128)(2,1)} %get-tuple-element.37) | copy-start | bytes 786436
  122.1 18.8 %collective-permute-start.5 = (bf16[64,2048]{1,0:T(8,128)(2,1)}, bf16[64,2048]{1,0:T(8,128)(2,1)S(1)}, u32[]{:S(2)}, u32[]{:S(2)}) collective-permute-start(bf16[64,2048]{1,0:T(8,128)(2,1)} %get-tuple-element.36), channel_id=1, source_target_pairs={{0,144},{16,160},{32,176},{48,128},{64,208},{80,224},{96,240},{112... | collective-permute-start | bytes 786440 | tf_op jit(solution)/shard_map/ppermute | solution.py:240
  129.4 18.1 %collective-permute-start.6 = (bf16[64,2048]{1,0:T(8,128)(2,1)S(1)}, bf16[64,2048]{1,0:T(8,128)(2,1)S(1)}, u32[]{:S(2)}, u32[]{:S(2)}) collective-permute-start(bf16[64,2048]{1,0:T(8,128)(2,1)S(1)} %copy-done.11), channel_id=1, source_target_pairs={{0,32},{16,48},{32,0},{48,16},{64,96},{80,112},{96,64},{112,80},{1... | collective-permute-start | bytes 786440 | tf_op jit(solution)/shard_map/ppermute | solution.py:240
  132.1 18.1 %collective-permute-start.10 = (bf16[64,2048]{1,0:T(8,128)(2,1)}, bf16[64,2048]{1,0:T(8,128)(2,1)S(1)}, u32[]{:S(2)}, u32[]{:S(2)}) collective-permute-start(bf16[64,2048]{1,0:T(8,128)(2,1)} %get-tuple-element.41), channel_id=1, source_target_pairs={{0,160},{16,176},{32,128},{48,144},{64,224},{80,240},{96,192},{112... | collective-permute-start | bytes 786440 | tf_op jit(solution)/shard_map/ppermute | solution.py:240
  138.4 14.8 %collective-permute-start.11 = (bf16[64,2048]{1,0:T(8,128)(2,1)}, bf16[64,2048]{1,0:T(8,128)(2,1)S(1)}, u32[]{:S(2)}, u32[]{:S(2)}) collective-permute-start(bf16[64,2048]{1,0:T(8,128)(2,1)} %get-tuple-element.42), channel_id=1, source_target_pairs={{0,240},{16,192},{32,208},{48,224},{64,48},{80,0},{96,16},{112,32}... | collective-permute-start | bytes 786440 | tf_op jit(solution)/shard_map/ppermute | solution.py:240
  139.4 15.3 %collective-permute-start.12 = (bf16[64,2048]{1,0:T(8,128)(2,1)}, bf16[64,2048]{1,0:T(8,128)(2,1)S(1)}, u32[]{:S(2)}, u32[]{:S(2)}) collective-permute-start(bf16[64,2048]{1,0:T(8,128)(2,1)} %get-tuple-element.43), channel_id=1, source_target_pairs={{0,80},{16,96},{32,112},{48,64},{64,144},{80,160},{96,176},{112,12... | collective-permute-start | bytes 786440 | tf_op jit(solution)/shard_map/ppermute | solution.py:240
  140.8 21.6 %collective-permute-start.13 = (bf16[64,2048]{1,0:T(8,128)(2,1)}, bf16[64,2048]{1,0:T(8,128)(2,1)S(1)}, u32[]{:S(2)}, u32[]{:S(2)}) collective-permute-start(bf16[64,2048]{1,0:T(8,128)(2,1)} %get-tuple-element.44), channel_id=1, source_target_pairs={{0,208},{16,224},{32,240},{48,192},{64,16},{80,32},{96,48},{112,0}... | collective-permute-start | bytes 786440 | tf_op jit(solution)/shard_map/ppermute | solution.py:240
  147.5 20.9 %collective-permute-start.14 = (bf16[64,2048]{1,0:T(8,128)(2,1)}, bf16[64,2048]{1,0:T(8,128)(2,1)}, u32[]{:S(2)}, u32[]{:S(2)}) collective-permute-start(bf16[64,2048]{1,0:T(8,128)(2,1)} %get-tuple-element.45), channel_id=1, source_target_pairs={{0,112},{16,64},{32,80},{48,96},{64,176},{80,128},{96,144},{112,16... | collective-permute-start | bytes 786440 | tf_op jit(solution)/shard_map/ppermute | solution.py:240
  150.3 21.4 %collective-permute-start = (bf16[64,2048]{1,0:T(8,128)(2,1)}, bf16[64,2048]{1,0:T(8,128)(2,1)}, u32[]{:S(2)}, u32[]{:S(2)}) collective-permute-start(bf16[64,2048]{1,0:T(8,128)(2,1)} %get-tuple-element.27), channel_id=1, source_target_pairs={{0,48},{16,0},{32,16},{48,32},{64,112},{80,64},{96,80},{112,96},{1... | collective-permute-start | bytes 786440 | tf_op jit(solution)/shard_map/ppermute | solution.py:240
  153.2 18.5 %collective-permute-start.1 = (bf16[64,2048]{1,0:T(8,128)(2,1)}, bf16[64,2048]{1,0:T(8,128)(2,1)}, u32[]{:S(2)}, u32[]{:S(2)}) collective-permute-start(bf16[64,2048]{1,0:T(8,128)(2,1)} %get-tuple-element.28), channel_id=1, source_target_pairs={{0,192},{16,208},{32,224},{48,240},{64,0},{80,16},{96,32},{112,48}... | collective-permute-start | bytes 786440 | tf_op jit(solution)/shard_map/ppermute | solution.py:240
  154.7 17.0 %collective-permute-start.2 = (bf16[64,2048]{1,0:T(8,128)(2,1)}, bf16[64,2048]{1,0:T(8,128)(2,1)}, u32[]{:S(2)}, u32[]{:S(2)}) collective-permute-start(bf16[64,2048]{1,0:T(8,128)(2,1)} %get-tuple-element.29), channel_id=1, source_target_pairs={{0,16},{16,32},{32,48},{48,0},{64,80},{80,96},{96,112},{112,64},{1... | collective-permute-start | bytes 786440 | tf_op jit(solution)/shard_map/ppermute | solution.py:240
  163.1 8.9 %collective-permute-start.3 = (bf16[64,2048]{1,0:T(8,128)(2,1)}, bf16[64,2048]{1,0:T(8,128)(2,1)}, u32[]{:S(2)}, u32[]{:S(2)}) collective-permute-start(bf16[64,2048]{1,0:T(8,128)(2,1)} %get-tuple-element.30), channel_id=1, source_target_pairs={{0,64},{16,80},{32,96},{48,112},{64,128},{80,144},{96,160},{112,17... | collective-permute-start | bytes 786440 | tf_op jit(solution)/shard_map/ppermute | solution.py:240
  163.1 2.3 %copy-start.3 = (bf16[256,2048]{1,0:T(8,128)(2,1)S(1)}, bf16[256,2048]{1,0:T(8,128)(2,1)}, u32[]{:S(2)}) copy-start(bf16[256,2048]{1,0:T(8,128)(2,1)} %get-tuple-element.46.normed_ref) | copy-start | bytes 3145732
  163.1 2.3 %copy-start.7 = (f32[2048]{0:T(1024)S(1)}, f32[2048]{0:T(1024)}, u32[]{:S(2)}) copy-start(f32[2048]{0:T(1024)} %param.23) | copy-start | bytes 24580
  168.5 3.4 %copy-start.6 = (bf16[64,2048]{1,0:T(8,128)(2,1)S(1)}, bf16[64,2048]{1,0:T(8,128)(2,1)}, u32[]{:S(2)}) copy-start(bf16[64,2048]{1,0:T(8,128)(2,1)} %get-tuple-element.31.refs_4_) | copy-start | bytes 786436
  (5 other events, 6.2 us)
Sparse Core Ops, SparseCore 0:
  9.2 79.7 all-gather.2
  90.8 39.0 all-gather.4
